TPU v7x, 32 devices: a whole 2x2x4 slice. The times are simulated.
32 devices in a mesh: grp: 2 (over y), kv: 4 (over z), tp: 4 (over x, core).
Axes of the slice: x: 2, y: 2, z: 4, core: 2. Of those that a mesh axis runs over, the one named last changes fastest.
Arguments:
- tokens: bfloat16 [256, 4096], P('grp', 'kv'), parts along dimension 0, may hold values from -36 to 36
- span_lengths: int32 [256], P(('grp', 'kv')), parts along dimension 0, may hold values from 1 to 256, 13107 in all
- block_state: float32 [256, 64, 32, 64], P(('grp', 'kv'), 'tp'), parts along dimension 0, may hold values from -96 to 96
- key_cache: bfloat16 [256, 2048, 256], P(('grp', 'kv'), 'tp'), parts along dimension 0, may hold values from -6 to 6
- value_cache: bfloat16 [256, 4096, 256], P(('grp', 'kv'), 'tp'), parts along dimension 0, may hold values from -6 to 6
- decay_cache: float32 [256, 2048, 256], P(('grp', 'kv'), 'tp'), parts along dimension 0, may hold values from -34 to 0, as said below
- attn_gain: float32 [4096], P('kv'), may hold values from 0.1 to 1.9
- query_weight: bfloat16 [4096, 2048], P('kv', 'tp'), may hold values from -0.09375 to 0.09375
- key_weight: bfloat16 [4096, 2048], P('kv', 'tp'), may hold values from -0.09375 to 0.09375
- value_weight: bfloat16 [4096, 4096], P('kv', 'tp'), may hold values from -0.09375 to 0.09375
- gate_weight: bfloat16 [4096, 4096], P('kv', 'tp'), may hold values from -0.09375 to 0.09375
- decay_matrix: bfloat16 [4096, 2048], P('kv', 'tp'), may hold values from -0.09375 to 0.09375
- decay_offset_bias: float32 [2048], P('tp'), may hold values from -1.4 to 6
- head_gain: float32 [64], replicated, may hold values from 0.1 to 1.9
- out_weight: bfloat16 [4096, 4096], P('tp', 'kv'), may hold values from -0.09375 to 0.09375
- mixer_gain: float32 [4096], P('kv'), may hold values from 0.1 to 1.9
- up_weight: bfloat16 [4096, 16384], P('kv', 'tp'), may hold values from -0.09375 to 0.09375
- down_weight: bfloat16 [16384, 4096], P('tp', 'kv'), may hold values from -0.046875 to 0.046875
Outputs:
- layer_out: bfloat16 [256, 4096], P('grp', 'kv'), parts along dimension 0
There are 2 independent parts, one for each index of `grp`. A program takes and returns all parts, laid end to end along the dimension named above; an argument that names none is the same for every part. Nothing has to cross between parts.
Inputs may be any that keep to these rules, and one draw needn't show every extreme that they name: Cached positions at index span_lengths - 1 and beyond are unused. `decay_cache`: Non-increasing along positions.
All inputs are finite; a program needn't handle non-finite values. No bound on the sum of `span_lengths` on one device may be relied on, other than what follows from the above.
Results may differ from a plain program's by a relative error of at most 0.005.
The roundings to bfloat16 on the way count: a program that leaves them out, or rounds other values in their place, can miss the bound.
Values may be sent and summed in bfloat16 or wider, within the bound.
A program may use at most 128 MiB of HBM per device.

v0:
```python
import jax
import jax.numpy as jnp
from jax import lax
from jax.sharding import PartitionSpec as P

D = 4096
KEY_WIDTH = 32
DV = 64
NORM_EPS = 1e-06
DECAY_SOFTNESS = 16.0


def shards(
    tokens,
    span_lengths,
    block_state,
    key_cache,
    value_cache,
    decay_cache,
    attn_gain,
    query_weight,
    key_weight,
    value_weight,
    gate_weight,
    decay_matrix,
    decay_offset_bias,
    head_gain,
    out_weight,
    mixer_gain,
    up_weight,
    down_weight,
):
    seq_count = block_state.shape[0]
    head_count = block_state.shape[1]
    span_size = key_cache.shape[2]
    whole_rows = tokens.astype(jnp.float32)
    square_sum = jnp.sum(whole_rows * whole_rows, axis=1)
    scaled = (whole_rows * attn_gain).astype(jnp.bfloat16)
    query_part = jnp.dot(scaled, query_weight, preferred_element_type=jnp.float32)
    key_part = jnp.dot(scaled, key_weight, preferred_element_type=jnp.float32)
    value_part = jnp.dot(scaled, value_weight, preferred_element_type=jnp.float32)
    gate_part = jnp.dot(scaled, gate_weight, preferred_element_type=jnp.float32)
    decay_part = jnp.dot(scaled, decay_matrix, preferred_element_type=jnp.float32)
    square_total = lax.psum(square_sum, "kv")
    query_sum, key_sum, value_sum, gate_sum, decay_running_sum = (
        lax.psum_scatter(query_part, "kv", scatter_dimension=0, tiled=True),
        lax.psum_scatter(key_part, "kv", scatter_dimension=0, tiled=True),
        lax.psum_scatter(value_part, "kv", scatter_dimension=0, tiled=True),
        lax.psum_scatter(gate_part, "kv", scatter_dimension=0, tiled=True),
        lax.psum_scatter(decay_part, "kv", scatter_dimension=0, tiled=True),
    )
    own_square = lax.dynamic_slice_in_dim(square_total, lax.axis_index("kv") * seq_count, seq_count)
    scale_per_row = lax.rsqrt(own_square / D + NORM_EPS)[:, None]
    query = (query_sum * scale_per_row * KEY_WIDTH ** (-0.5)).reshape(
        seq_count, head_count, KEY_WIDTH
    )
    key_new = (key_sum * scale_per_row).reshape(seq_count, head_count, KEY_WIDTH)
    value_new = (value_sum * scale_per_row).reshape(seq_count, head_count, DV)
    gate = gate_sum * scale_per_row
    logarithm_decay = (
        jax.nn.log_sigmoid(decay_running_sum * scale_per_row + decay_offset_bias) / DECAY_SOFTNESS
    )
    token_place = lax.broadcasted_iota(jnp.int32, (1, 1, span_size), 2)
    lengths_now = span_lengths[:, None, None]
    previous = jnp.sum(jnp.where(token_place == lengths_now - 2, decay_cache, 0.0), axis=-1)
    now_decay = (previous + logarithm_decay).reshape(seq_count, head_count, KEY_WIDTH)
    decays_span = decay_cache.reshape(seq_count, head_count, KEY_WIDTH, span_size)
    in_use = (token_place < lengths_now - 1)[:, :, None, :]
    factor = jnp.where(in_use, jnp.exp(now_decay[..., None] - decays_span), 0.0)
    keys_span = key_cache.reshape(seq_count, head_count, KEY_WIDTH, span_size)
    scores = jnp.sum(query[..., None] * keys_span.astype(jnp.float32) * factor, axis=2)
    scores_low = scores.astype(jnp.bfloat16)
    values_span = value_cache.reshape(seq_count, head_count, DV, span_size)
    history = jnp.einsum(
        "nhs,nhvs->nhv", scores_low, values_span, preferred_element_type=jnp.float32
    )
    carried = jnp.einsum(
        "nhc,nhcv->nhv", query * jnp.exp(now_decay), block_state, precision=lax.Precision.HIGHEST
    )
    own_term = jnp.sum(query * key_new, axis=-1, keepdims=True) * value_new
    raw = carried + history + own_term
    normed = raw * lax.rsqrt(jnp.mean(raw * raw, axis=-1, keepdims=True) + NORM_EPS) * head_gain
    mixed = (normed.reshape(seq_count, head_count * DV) * jax.nn.silu(gate)).astype(jnp.bfloat16)
    attn_terms = jnp.dot(
        lax.all_gather(mixed, "kv", axis=0, tiled=True),
        out_weight,
        preferred_element_type=jnp.float32,
    )
    attn_out = lax.psum(attn_terms, "tp")
    resid = (whole_rows + attn_out).astype(jnp.bfloat16)
    resid_rows = resid.astype(jnp.float32)
    mixer_square = jnp.sum(resid_rows * resid_rows, axis=1)
    mixer_scaled = (resid_rows * mixer_gain).astype(jnp.bfloat16)
    up_part = jnp.dot(mixer_scaled, up_weight, preferred_element_type=jnp.float32)
    up_share, square_share = (
        lax.psum_scatter(up_part, "kv", scatter_dimension=0, tiled=True),
        lax.psum_scatter(mixer_square, "kv", scatter_dimension=0, tiled=True),
    )
    hidden_share = jnp.square(
        jax.nn.relu(up_share * lax.rsqrt(square_share / D + NORM_EPS)[:, None])
    )
    hidden_share = hidden_share.astype(jnp.bfloat16)
    down_terms = jnp.dot(
        lax.all_gather(hidden_share, "kv", axis=0, tiled=True),
        down_weight,
        preferred_element_type=jnp.float32,
    )
    mixer_out = lax.psum(down_terms, "tp")
    return (resid_rows + mixer_out).astype(jnp.bfloat16)


def solution(mesh):
    placed = (
        P("grp", "kv"),
        P(("grp", "kv")),
        P(("grp", "kv"), "tp", None, None),
        P(("grp", "kv"), "tp", None),
        P(("grp", "kv"), "tp", None),
        P(("grp", "kv"), "tp", None),
        P("kv"),
        P("kv", "tp"),
        P("kv", "tp"),
        P("kv", "tp"),
        P("kv", "tp"),
        P("kv", "tp"),
        P("tp"),
        P(),
        P("tp", "kv"),
        P("kv"),
        P("kv", "tp"),
        P("tp", "kv"),
    )
    return jax.shard_map(
        shards, mesh=mesh, in_specs=placed, out_specs=P("grp", "kv"), check_vma=False
    )
```

profile of v0, /device:TPU:0, one launch (start us, length us, event | category | flops | bytes accessed | tf_op | source)
XLA Modules:
  0.0 293.3 jit_solution(13781271329002494492)
XLA Ops:
  6.6 2.5 fusion.21
  9.1 0.0 reduce-scatter.11.cloned.1.call-start
  9.2 2.4 fusion.17
  11.6 2.3 fusion.19
  14.0 0.0 reduce-scatter.13.cloned.1.call-start
  14.0 2.2 fusion.15
  16.2 0.0 reduce-scatter.15.cloned.1.call-start
  16.3 2.9 fusion.13
  19.2 0.0 all-reduce.4.cloned.1.call-start
  19.2 0.1 fusion.3
  19.4 13.6 %psum.21 = f32[128]{0:T(128)S(1)} all-reduce(f32[128]{0:T(128)S(1)} %fusion.3), channel_id=1, replica_groups=mesh['grp'=2,'kv'=4,'tp'=4] {'kv'}, use_global_device_ids=true, to_apply=%region_2.0 | all-reduce | flops 128 | bytes 1024 | tf_op jit(solution)/shard_map/psum | solution.py:44
  33.0 0.1 iota_compare_fusion
  33.0 0.1 iota_compare_fusion.1
  33.1 0.1 add_rsqrt_fusion.1
  33.2 8.0 %select_reduce_fusion = f32[32,512]{1,0:T(8,128)S(1)} fusion(f32[32,512,256]{2,1,0:T(8,128)} %param.23, pred[32,256]{1,0:T(8,128)(4,1)S(1)} %iota_compare_fusion.1), kind=kLoop, calls=%fused_computation.3 | loop fusion | flops 8372224 | bytes 16850944 | tf_op jit(solution)/shard_map/reduce_sum | solution.py:65
  41.3 11.6 %reduce-scatter.11.cloned.1.call-done = f32[32,512]{1,0:T(8,128)} async-done(((f32[128,512]{1,0:T(8,128)}), f32[32,512]{1,0:T(8,128)}) %reduce-scatter.11.cloned.1.call-update) | async-done | bytes 65552 | tf_op jit(solution)/shard_map/reduce_scatter | solution.py:47
  52.9 20.5 %reduce-scatter.9.cloned.1.call-done = f32[32,512]{1,0:T(8,128)} async-done(((f32[128,512]{1,0:T(8,128)}), f32[32,512]{1,0:T(8,128)}) %reduce-scatter.9.cloned.1.call-update) | async-done | bytes 65552 | tf_op jit(solution)/shard_map/reduce_scatter | solution.py:50
  73.5 1.0 fusion.25
  74.5 0.1 reshape.83
  74.6 0.1 reshape.82
  74.7 0.1 reshape.86
  74.8 0.1 exponential_multiply_fusion
  75.0 9.7 %fusion.1 = bf16[32,16,256]{2,1,0:T(8,128)(2,1)S(1)} fusion(f32[32,16,32]{2,1,0:T(8,128)S(1)} %reshape.83, f32[32,16,32]{2,1,0:T(8,128)S(1)} %reshape.82, pred[32,256]{1,0:T(8,128)(4,1)S(1)} %iota_compare_fusion, bf16[32,512,256]{2,1,0:T(8,128)(2,1)} %param.21, f32[32,512,256]{2,1,0:T(8,128)} %param.23), kind=kLoop, calls=%fused_computation.2 | loop fusion | flops 25034752 | bytes 25567232 | tf_op jit(solution)/shard_map/reduce_sum | solution.py:71
  84.7 10.3 %fusion.8 = f32[32,16,1,64]{3,2,1,0:T(1,128)S(1)} fusion(bf16[32,16,64,256]{3,2,1,0:T(8,128)(2,1)} %bitcast.34, bf16[32,16,256,1]{2,1,0,3:T(8,128)(2,1)S(1)} %bitcast.32), kind=kOutput, calls=%fused_computation.16 | convolution fusion | flops 16777216 | bytes 17170432 | tf_op jit(solution)/shard_map/nhs,nhvs->nhv/dot_general | solution.py:74
  94.9 9.2 %fusion.29 = f32[32,16,1,64]{3,2,1,0:T(1,128)S(1)} fusion(f32[32,16,32,1]{2,3,1,0:T(1,128)S(1)} %bitcast.31, f32[32,16,32,64]{3,2,1,0:T(8,128)} %param.20), kind=kOutput, calls=%fused_computation.49 | convolution fusion | flops 12582912 | bytes 4390912 | tf_op jit(solution)/shard_map/nhc,nhcv->nhv/dot_general | solution.py:77
  104.2 1.0 broadcast_multiply_fusion
  105.2 0.1 reshape.87
  105.3 0.2 multiply_reduce_fusion
  105.6 0.1 multiply_multiply_fusion
  105.7 0.1 reshape.88
  105.8 12.1 %reduce-scatter.15.cloned.1.call-done = f32[32,1024]{1,0:T(8,128)} async-done(((f32[128,1024]{1,0:T(8,128)}), f32[32,1024]{1,0:T(8,128)}) %reduce-scatter.15.cloned.1.call-update) | async-done | bytes 131088 | tf_op jit(solution)/shard_map/reduce_scatter | solution.py:49
  118.0 1.0 multiply_convert_fusion.1
  119.0 13.8 %all_gather.6 = bf16[128,1024]{1,0:T(8,128)(2,1)S(1)} all-gather(bf16[32,1024]{1,0:T(8,128)(2,1)S(1)} %multiply_convert_fusion.1), channel_id=1, replica_groups=mesh['grp'=2,'kv'=4,'tp'=4] {'kv'}, dimensions={0}, use_global_device_ids=true | all-gather | bytes 327680 | tf_op jit(solution)/shard_map/all_gather | solution.py:85
  132.8 1.3 fusion.30
  134.1 0.2 reduce-scatter.17.cloned.1.call-start
  134.3 31.5 %all-reduce.4.cloned.1.call-done = f32[128,1024]{1,0:T(8,128)} async-done(((f32[128,1024]{1,0:T(8,128)}), f32[128,1024]{1,0:T(8,128)}) %all-reduce.4.cloned.1.call-update) | async-done | bytes 524304 | tf_op jit(solution)/shard_map/psum | solution.py:89
  165.8 1.2 fusion.6
  167.0 6.0 %fusion.10 = f32[128,4096]{1,0:T(8,128)} fusion(bf16[1024,4096]{1,0:T(8,128)(2,1)} %param.34, bf16[128,1024]{1,0:T(8,128)(2,1)S(1)} %get-tuple-element.6, f32[1024]{0:T(1024)S(1)} %copy-done.5), kind=kOutput, calls=%fused_computation.19 | convolution fusion | flops 1074135040 | bytes 10752000 | tf_op jit(solution)/shard_map/dot_general | solution.py:94
  173.1 0.0 all-gather.2.cloned.1.call-start
  173.1 0.6 dynamic-slice
  174.4 12.1 %all-reduce = f32[128]{0:T(128)S(1)} all-reduce(f32[128]{0:T(128)S(1)} %get-tuple-element.5), channel_id=8, replica_groups=mesh['grp'=2,'kv'=4,'tp'=4] {'kv'}, use_global_device_ids=true, to_apply=%region_14.15.clone | all-reduce | flops 128 | bytes 1024
  186.4 0.1 fusion.27
  186.5 30.4 %reduce-scatter.17.cloned.1.call-done = f32[32,4096]{1,0:T(8,128)} async-done(((f32[128,4096]{1,0:T(8,128)}), f32[32,4096]{1,0:T(8,128)}) %reduce-scatter.17.cloned.1.call-update) | async-done | bytes 524304 | tf_op jit(solution)/shard_map/reduce_scatter | solution.py:96
  217.0 1.9 multiply_convert_fusion
  218.9 27.3 %all-gather.2.cloned.1.call-done = bf16[128,4096]{1,0:T(8,128)(2,1)} async-done(((bf16[32,4096]{1,0:T(8,128)(2,1)}), bf16[128,4096]{1,0:T(8,128)(2,1)}) %all-gather.2.cloned.1.call-update) | async-done | bytes 1048592 | tf_op jit(solution)/shard_map/all_gather | solution.py:104
  246.2 5.8 %fusion.31 = f32[128,1024]{1,0:T(8,128)} fusion(bf16[128,4096]{1,0:T(8,128)(2,1)} %all-gather.2.cloned.1.call-done, bf16[4096,1024]{1,0:T(8,128)(2,1)} %param.35), kind=kOutput, calls=%fused_computation.51 | convolution fusion | flops 1073741824 | bytes 9961472 | tf_op jit(solution)/shard_map/dot_general | solution.py:103
  252.0 32.9 %all-reduce.6.cloned.1.call-done = f32[128,1024]{1,0:T(8,128)} async-done(((f32[128,1024]{1,0:T(8,128)}), f32[128,1024]{1,0:T(8,128)}) %all-reduce.6.cloned.1.call-update) | async-done | bytes 524304 | tf_op jit(solution)/shard_map/psum | solution.py:108
  284.9 1.8 fusion.7
  (36 shorter events, 0.4 us)
Async XLA Ops:
  6.5 7.5 %copy-start = (bf16[1024,1024]{1,0:T(8,128)(2,1)S(1)}, bf16[1024,1024]{1,0:T(8,128)(2,1)}, u32[]{:S(2)}) copy-start(bf16[1024,1024]{1,0:T(8,128)(2,1)} %param.27) | copy-start | bytes 6291460
  6.5 9.8 %copy-start.2 = (bf16[128,1024]{1,0:T(8,128)(2,1)S(1)}, bf16[128,1024]{1,0:T(8,128)(2,1)}, u32[]{:S(2)}) copy-start(bf16[128,1024]{1,0:T(8,128)(2,1)} %param.18) | copy-start | bytes 786436
  6.5 9.8 %copy-start.4 = (f32[1024]{0:T(1024)S(1)}, f32[1024]{0:T(1024)}, u32[]{:S(2)}) copy-start(f32[1024]{0:T(1024)} %param.24) | copy-start | bytes 12292
  6.5 26.4 %copy-start.8 = (s32[32]{0:T(128)S(1)}, s32[32]{0:T(128)}, u32[]{:S(2)}) copy-start(s32[32]{0:T(128)} %param.19) | copy-start | bytes 388
  6.5 34.7 %reduce-scatter.7.cloned.1.call-start = ((), (), s32[]{:S(2)}) async-start(), calls=%async_computation.6 | async-start | bytes 327680 | tf_op jit(solution)/shard_map/reduce_scatter | solution.py:46
  9.1 43.8 %reduce-scatter.11.cloned.1.call-start = ((), (), s32[]{:S(2)}) async-start(), calls=%async_computation.8 | async-start | bytes 327680 | tf_op jit(solution)/shard_map/reduce_scatter | solution.py:47
  11.5 61.9 %reduce-scatter.9.cloned.1.call-start = ((), (), s32[]{:S(2)}) async-start(), calls=%async_computation.7 | async-start | bytes 327680 | tf_op jit(solution)/shard_map/reduce_scatter | solution.py:50
  14.0 90.2 %reduce-scatter.13.cloned.1.call-start = ((), (), s32[]{:S(2)}) async-start(), calls=%async_computation.9 | async-start | bytes 655360 | tf_op jit(solution)/shard_map/reduce_scatter | solution.py:48
  16.2 101.7 %reduce-scatter.15.cloned.1.call-start = ((), (), s32[]{:S(2)}) async-start(), calls=%async_computation.10 | async-start | bytes 655360 | tf_op jit(solution)/shard_map/reduce_scatter | solution.py:49
  19.2 146.6 %all-reduce.4.cloned.1.call-start = ((), (), s32[]{:S(2)}) async-start(), calls=%async_computation.11 | async-start | bytes 1048576 | tf_op jit(solution)/shard_map/psum | solution.py:89
  33.2 40.2 %copy-start.6 = (f32[512]{0:T(512)S(1)}, f32[512]{0:T(512)}, u32[]{:S(2)}) copy-start(f32[512]{0:T(512)} %param.30) | copy-start | bytes 6148
  94.9 10.6 %copy-start.7 = (f32[64]{0:T(128)S(1)}, f32[64]{0:T(128)}, u32[]{:S(2)}) copy-start(f32[64]{0:T(128)} %param.31) | copy-start | bytes 772
  94.9 37.9 %copy-start.3 = (bf16[1024,1024]{1,0:T(8,128)(2,1)S(1)}, bf16[1024,1024]{1,0:T(8,128)(2,1)}, u32[]{:S(2)}) copy-start(bf16[1024,1024]{1,0:T(8,128)(2,1)} %param.32) | copy-start | bytes 6291460
  94.9 72.1 %copy-start.5 = (f32[1024]{0:T(1024)S(1)}, f32[1024]{0:T(1024)}, u32[]{:S(2)}) copy-start(f32[1024]{0:T(1024)} %param.33) | copy-start | bytes 12292
  134.1 82.9 %reduce-scatter.17.cloned.1.call-start = ((), (), s32[]{:S(2)}) async-start(), calls=%async_computation.12 | async-start | bytes 2621440 | tf_op jit(solution)/shard_map/reduce_scatter | solution.py:96
  167.0 6.1 %copy-start.9 = (u32[32]{0:T(128)S(1)}, u32[32]{0:T(128)}, u32[]{:S(2)}) copy-start(u32[32]{0:T(128)} %constant.44) | copy-start | bytes 388
  173.1 73.1 %all-gather.2.cloned.1.call-start = ((), (), s32[]{:S(2)}) async-start(), calls=%async_computation.13 | async-start | bytes 1310720 | tf_op jit(solution)/shard_map/all_gather | solution.py:104
  218.9 67.9 %copy-start.1 = (bf16[1024,1024]{1,0:T(8,128)(2,1)S(1)}, bf16[1024,1024]{1,0:T(8,128)(2,1)}, u32[]{:S(2)}) copy-start(bf16[1024,1024]{1,0:T(8,128)(2,1)} %param.27) | copy-start | bytes 6291460
  218.9 66.1 %all-reduce.6.cloned.1.call-start = ((), (), s32[]{:S(2)}) async-start(), calls=%async_computation.14 | async-start | bytes 1048576 | tf_op jit(solution)/shard_map/psum | solution.py:108
Sparse Core Ops, SparseCore 0:
  9.6 22.7 reduce-scatter.6
  34.6 18.2 reduce-scatter.10
  55.2 18.2 reduce-scatter.8
  75.6 20.1 reduce-scatter.12
  97.8 20.0 reduce-scatter.14
  134.2 31.5 all-reduce.3
  173.2 43.7 reduce-scatter.16
  219.0 27.1 all-gather.1
  252.1 32.7 all-reduce.5
where the time goes:
time: 294 us; the launch traced here: 293 us
  waiting for transfers between devices  167 us (57%)
  matrix products  44.8 us (15%)
  blocking collectives  39.5 us (13%)
  other arithmetic  26.6 us (9%)
  between operations  14 us (5%)
    psum x1, waiting for transfers between devices, shards(): mixer_out = lax.psum(down_terms, 'tp')  32.9 us
    psum x1, waiting for transfers between devices, shards(): attn_out = lax.psum(attn_terms, 'tp')  31.5 us
    reduce_scatter x1, waiting for transfers between devices, shards(): lax.psum_scatter(up_part, 'kv', scatter_dimension=0, tiled=True)  30.4 us
    all_gather x1, waiting for transfers between devices, shards(): lax.all_gather(hidden_share, 'kv', axis=0, tiled=True)  27.3 us
    reduce_scatter x1, waiting for transfers between devices, shards(): lax.psum_scatter(decay_part, 'kv', scatter_dimension=0, tiled=True)  20.5 us
    all_gather x1, blocking collectives, shards(): lax.all_gather(mixed, 'kv', axis=0, tiled=True)  13.8 us
    psum x1, blocking collectives, shards(): square_total = lax.psum(square_sum, 'kv')  13.6 us
    reduce_scatter x1, waiting for transfers between devices, shards(): lax.psum_scatter(gate_part, 'kv', scatter_dimension=0, tiled=True)  12.1 us
  transfers between devices with their start and end apart: 9, of which 7 were waited for; matrix products, arithmetic and copies ran while one was open for 17% of the time, Pallas kernels for 0%

commit v1 on v0

--- a/solution.py
+++ b/solution.py
@@ -86,7 +86,9 @@
         out_weight,
         preferred_element_type=jnp.float32,
     )
-    attn_out = lax.psum(attn_terms, "tp")
+    attn_out = attn_terms
+    for hop in (1, 2):
+        attn_out = attn_out + lax.ppermute(attn_out, "tp", [(dev, dev ^ hop) for dev in range(4)])
     resid = (whole_rows + attn_out).astype(jnp.bfloat16)
     resid_rows = resid.astype(jnp.float32)
     mixer_square = jnp.sum(resid_rows * resid_rows, axis=1)

time: 294 us -> 275 us (0.935)
  waiting for transfers between devices: 167 us -> 151 us
  blocking collectives: 39.5 us -> 36.5 us
    psum x1 -> x0, waiting for transfers between devices: 31.5 us -> none  [shards(): attn_out = lax.psum(attn_terms, 'tp')]
    ppermute x0 -> x2, waiting for transfers between devices: none -> 14.4 us  [shards(): lax.ppermute(attn_out, 'tp', [(dev, dev ^ hop) for dev in range(4)])]
    unnamed x1, blocking collectives: 12.1 us -> 8.98 us
  transfers between devices with their start and end apart: 9 -> 10, of which waited for: 7 -> 8; matrix products, arithmetic and copies ran while one was open for 17% -> 19% of each run, Pallas kernels for 0% -> 0%
where the time goes in v1:
time: 275 us; the launch traced here: 274 us
  waiting for transfers between devices  151 us (55%)
  matrix products  44 us (16%)
  blocking collectives  36.5 us (13%)
  other arithmetic  25.6 us (9%)
  between operations  14.4 us (5%)
    psum x1, waiting for transfers between devices, shards(): mixer_out = lax.psum(down_terms, 'tp')  32.9 us
    reduce_scatter x1, waiting for transfers between devices, shards(): lax.psum_scatter(up_part, 'kv', scatter_dimension=0, tiled=True)  31.6 us
    all_gather x1, waiting for transfers between devices, shards(): lax.all_gather(hidden_share, 'kv', axis=0, tiled=True)  27.3 us
    reduce_scatter x1, waiting for transfers between devices, shards(): lax.psum_scatter(decay_part, 'kv', scatter_dimension=0, tiled=True)  20.5 us
    ppermute x2, waiting for transfers between devices, shards(): lax.ppermute(attn_out, 'tp', [(dev, dev ^ hop) for dev in range(4)])  14.4 us
    all_gather x1, blocking collectives, shards(): lax.all_gather(mixed, 'kv', axis=0, tiled=True)  14 us
    psum x1, blocking collectives, shards(): square_total = lax.psum(square_sum, 'kv')  13.6 us
    reduce_scatter x1, waiting for transfers between devices, shards(): lax.psum_scatter(gate_part, 'kv', scatter_dimension=0, tiled=True)  12.1 us
  transfers between devices with their start and end apart: 10, of which 8 were waited for; matrix products, arithmetic and copies ran while one was open for 19% of the time, Pallas kernels for 0%

profile of v1, /device:TPU:0, one launch (start us, length us, event | category | flops | bytes accessed | tf_op | source)
XLA Modules:
  0.0 274.3 jit_solution(16540201385664376728)
XLA Ops:
  6.6 2.5 fusion.21
  9.1 0.0 reduce-scatter.11.cloned.1.call-start
  9.2 2.4 fusion.17
  11.6 2.3 fusion.19
  14.0 2.2 fusion.15
  16.3 2.9 %fusion.13 = f32[128,1024]{1,0:T(8,128)} fusion(bf16[1024,1024]{1,0:T(8,128)(2,1)} %param.28, bf16[128,1024]{1,0:T(8,128)(2,1)S(1)} %copy-done.2, f32[1024]{0:T(1024)S(1)} %copy-done.4), kind=kOutput, calls=%fused_computation.29 | convolution fusion | flops 268828672 | bytes 2887680 | tf_op jit(solution)/shard_map/dot_general | solution.py:42
  19.2 0.1 fusion.3
  19.4 13.6 %psum.14 = f32[128]{0:T(128)S(1)} all-reduce(f32[128]{0:T(128)S(1)} %fusion.3), channel_id=1, replica_groups=mesh['grp'=2,'kv'=4,'tp'=4] {'kv'}, use_global_device_ids=true, to_apply=%region_2.0 | all-reduce | flops 128 | bytes 1024 | tf_op jit(solution)/shard_map/psum | solution.py:44
  33.0 0.1 iota_compare_fusion
  33.0 0.1 iota_compare_fusion.1
  33.1 0.1 add_rsqrt_fusion.1
  33.2 8.0 %select_reduce_fusion = f32[32,512]{1,0:T(8,128)S(1)} fusion(f32[32,512,256]{2,1,0:T(8,128)} %param.23, pred[32,256]{1,0:T(8,128)(4,1)S(1)} %iota_compare_fusion.1), kind=kLoop, calls=%fused_computation.3 | loop fusion | flops 8372224 | bytes 16850944 | tf_op jit(solution)/shard_map/reduce_sum | solution.py:65
  41.3 11.6 %reduce-scatter.11.cloned.1.call-done = f32[32,512]{1,0:T(8,128)} async-done(((f32[128,512]{1,0:T(8,128)}), f32[32,512]{1,0:T(8,128)}) %reduce-scatter.11.cloned.1.call-update) | async-done | bytes 65552 | tf_op jit(solution)/shard_map/reduce_scatter | solution.py:47
  52.9 20.5 %reduce-scatter.9.cloned.1.call-done = f32[32,512]{1,0:T(8,128)} async-done(((f32[128,512]{1,0:T(8,128)}), f32[32,512]{1,0:T(8,128)}) %reduce-scatter.9.cloned.1.call-update) | async-done | bytes 65552 | tf_op jit(solution)/shard_map/reduce_scatter | solution.py:50
  73.5 1.0 fusion.25
  74.5 0.1 reshape.83
  74.6 0.1 reshape.82
  74.7 0.1 reshape.86
  74.8 0.1 exponential_multiply_fusion
  75.0 9.7 %fusion.1 = bf16[32,16,256]{2,1,0:T(8,128)(2,1)S(1)} fusion(f32[32,16,32]{2,1,0:T(8,128)S(1)} %reshape.83, f32[32,16,32]{2,1,0:T(8,128)S(1)} %reshape.82, pred[32,256]{1,0:T(8,128)(4,1)S(1)} %iota_compare_fusion, bf16[32,512,256]{2,1,0:T(8,128)(2,1)} %param.21, f32[32,512,256]{2,1,0:T(8,128)} %param.23), kind=kLoop, calls=%fused_computation.2 | loop fusion | flops 25034752 | bytes 25567232 | tf_op jit(solution)/shard_map/reduce_sum | solution.py:71
  84.7 10.3 %fusion.8 = f32[32,16,1,64]{3,2,1,0:T(1,128)S(1)} fusion(bf16[32,16,64,256]{3,2,1,0:T(8,128)(2,1)} %bitcast.34, bf16[32,16,256,1]{2,1,0,3:T(8,128)(2,1)S(1)} %bitcast.32), kind=kOutput, calls=%fused_computation.16 | convolution fusion | flops 16777216 | bytes 17170432 | tf_op jit(solution)/shard_map/nhs,nhvs->nhv/dot_general | solution.py:74
  94.9 9.2 %fusion.29 = f32[32,16,1,64]{3,2,1,0:T(1,128)S(1)} fusion(f32[32,16,32,1]{2,3,1,0:T(1,128)S(1)} %bitcast.31, f32[32,16,32,64]{3,2,1,0:T(8,128)} %param.20), kind=kOutput, calls=%fused_computation.49 | convolution fusion | flops 12582912 | bytes 4390912 | tf_op jit(solution)/shard_map/nhc,nhcv->nhv/dot_general | solution.py:77
  104.2 1.0 broadcast_multiply_fusion
  105.2 0.1 reshape.87
  105.3 0.2 multiply_reduce_fusion
  105.6 0.1 multiply_multiply_fusion
  105.7 0.1 reshape.88
  105.8 12.1 %reduce-scatter.15.cloned.1.call-done = f32[32,1024]{1,0:T(8,128)} async-done(((f32[128,1024]{1,0:T(8,128)}), f32[32,1024]{1,0:T(8,128)}) %reduce-scatter.15.cloned.1.call-update) | async-done | bytes 131088 | tf_op jit(solution)/shard_map/reduce_scatter | solution.py:49
  118.0 1.0 multiply_convert_fusion.1
  119.0 14.0 %all_gather.6 = bf16[128,1024]{1,0:T(8,128)(2,1)S(1)} all-gather(bf16[32,1024]{1,0:T(8,128)(2,1)S(1)} %multiply_convert_fusion.1), channel_id=1, replica_groups=mesh['grp'=2,'kv'=4,'tp'=4] {'kv'}, dimensions={0}, use_global_device_ids=true | all-gather | bytes 327680 | tf_op jit(solution)/shard_map/all_gather | solution.py:85
  133.0 0.4 fusion.30
  133.4 0.1 collective-permute-start
  133.5 1.9 collective-permute-done
  135.4 0.1 add.91
  135.5 1.5 collective-permute-start.1
  137.0 12.5 %collective-permute-done.1 = f32[128,1024]{1,0:T(8,128)S(1)} collective-permute-done((f32[128,1024]{1,0:T(8,128)S(1)}, f32[128,1024]{1,0:T(8,128)S(1)}, u32[]{:S(2)}, u32[]{:S(2)}) %collective-permute-start.1) | collective-permute-done | bytes 524320 | tf_op jit(solution)/shard_map/ppermute | solution.py:91
  149.5 0.2 fusion.6
  149.7 6.0 %fusion.10 = f32[128,4096]{1,0:T(8,128)} fusion(bf16[1024,4096]{1,0:T(8,128)(2,1)} %param.34, bf16[128,1024]{1,0:T(8,128)(2,1)S(1)} %get-tuple-element.6, f32[1024]{0:T(1024)S(1)} %copy-done.5), kind=kOutput, calls=%fused_computation.19 | convolution fusion | flops 1074135040 | bytes 10752000 | tf_op jit(solution)/shard_map/dot_general | solution.py:96
  155.8 0.6 dynamic-slice
  157.0 9.0 %all-reduce = f32[128]{0:T(128)S(1)} all-reduce(f32[128]{0:T(128)S(1)} %get-tuple-element.5), channel_id=8, replica_groups=mesh['grp'=2,'kv'=4,'tp'=4] {'kv'}, use_global_device_ids=true, to_apply=%region_13.14.clone | all-reduce | flops 128 | bytes 1024
  166.0 0.1 fusion.27
  166.1 31.6 %reduce-scatter.17.cloned.1.call-done = f32[32,4096]{1,0:T(8,128)} async-done(((f32[128,4096]{1,0:T(8,128)}), f32[32,4096]{1,0:T(8,128)}) %reduce-scatter.17.cloned.1.call-update) | async-done | bytes 524304 | tf_op jit(solution)/shard_map/reduce_scatter | solution.py:98
  197.7 1.9 multiply_convert_fusion
  199.6 0.0 all-reduce.3.cloned.1.call-start
  199.6 27.3 %all-gather.2.cloned.1.call-done = bf16[128,4096]{1,0:T(8,128)(2,1)} async-done(((bf16[32,4096]{1,0:T(8,128)(2,1)}), bf16[128,4096]{1,0:T(8,128)(2,1)}) %all-gather.2.cloned.1.call-update) | async-done | bytes 1048592 | tf_op jit(solution)/shard_map/all_gather | solution.py:106
  226.9 5.8 %fusion.31 = f32[128,1024]{1,0:T(8,128)} fusion(bf16[128,4096]{1,0:T(8,128)(2,1)} %all-gather.2.cloned.1.call-done, bf16[4096,1024]{1,0:T(8,128)(2,1)} %param.35), kind=kOutput, calls=%fused_computation.51 | convolution fusion | flops 1073741824 | bytes 9961472 | tf_op jit(solution)/shard_map/dot_general | solution.py:105
  232.7 32.9 %all-reduce.3.cloned.1.call-done = f32[128,1024]{1,0:T(8,128)} async-done(((f32[128,1024]{1,0:T(8,128)}), f32[128,1024]{1,0:T(8,128)}) %all-reduce.3.cloned.1.call-update) | async-done | bytes 524304 | tf_op jit(solution)/shard_map/psum | solution.py:110
  265.7 1.8 fusion.7
  (38 shorter events, 0.5 us)
Async XLA Ops:
  6.5 7.5 %copy-start = (bf16[1024,1024]{1,0:T(8,128)(2,1)S(1)}, bf16[1024,1024]{1,0:T(8,128)(2,1)}, u32[]{:S(2)}) copy-start(bf16[1024,1024]{1,0:T(8,128)(2,1)} %param.27) | copy-start | bytes 6291460
  6.5 9.8 %copy-start.2 = (bf16[128,1024]{1,0:T(8,128)(2,1)S(1)}, bf16[128,1024]{1,0:T(8,128)(2,1)}, u32[]{:S(2)}) copy-start(bf16[128,1024]{1,0:T(8,128)(2,1)} %param.18) | copy-start | bytes 786436
  6.5 9.8 %copy-start.4 = (f32[1024]{0:T(1024)S(1)}, f32[1024]{0:T(1024)}, u32[]{:S(2)}) copy-start(f32[1024]{0:T(1024)} %param.24) | copy-start | bytes 12292
  6.5 26.4 %copy-start.8 = (s32[32]{0:T(128)S(1)}, s32[32]{0:T(128)}, u32[]{:S(2)}) copy-start(s32[32]{0:T(128)} %param.19) | copy-start | bytes 388
  6.5 34.7 %reduce-scatter.7.cloned.1.call-start = ((), (), s32[]{:S(2)}) async-start(), calls=%async_computation.6 | async-start | bytes 327680 | tf_op jit(solution)/shard_map/reduce_scatter | solution.py:46
  9.1 43.8 %reduce-scatter.11.cloned.1.call-start = ((), (), s32[]{:S(2)}) async-start(), calls=%async_computation.8 | async-start | bytes 327680 | tf_op jit(solution)/shard_map/reduce_scatter | solution.py:47
  11.5 61.9 %reduce-scatter.9.cloned.1.call-start = ((), (), s32[]{:S(2)}) async-start(), calls=%async_computation.7 | async-start | bytes 327680 | tf_op jit(solution)/shard_map/reduce_scatter | solution.py:50
  14.0 90.2 %reduce-scatter.13.cloned.1.call-start = ((), (), s32[]{:S(2)}) async-start(), calls=%async_computation.9 | async-start | bytes 655360 | tf_op jit(solution)/shard_map/reduce_scatter | solution.py:48
  16.2 101.7 %reduce-scatter.15.cloned.1.call-start = ((), (), s32[]{:S(2)}) async-start(), calls=%async_computation.10 | async-start | bytes 655360 | tf_op jit(solution)/shard_map/reduce_scatter | solution.py:49
  19.2 178.5 %reduce-scatter.17.cloned.1.call-start = ((), (), s32[]{:S(2)}) async-start(), calls=%async_computation.11 | async-start | bytes 2621440 | tf_op jit(solution)/shard_map/reduce_scatter | solution.py:98
  33.2 40.2 %copy-start.6 = (f32[512]{0:T(512)S(1)}, f32[512]{0:T(512)}, u32[]{:S(2)}) copy-start(f32[512]{0:T(512)} %param.30) | copy-start | bytes 6148
  94.9 10.6 %copy-start.7 = (f32[64]{0:T(128)S(1)}, f32[64]{0:T(128)}, u32[]{:S(2)}) copy-start(f32[64]{0:T(128)} %param.31) | copy-start | bytes 772
  94.9 38.0 %copy-start.3 = (bf16[1024,1024]{1,0:T(8,128)(2,1)S(1)}, bf16[1024,1024]{1,0:T(8,128)(2,1)}, u32[]{:S(2)}) copy-start(bf16[1024,1024]{1,0:T(8,128)(2,1)} %param.32) | copy-start | bytes 6291460
  94.9 54.7 %copy-start.5 = (f32[1024]{0:T(1024)S(1)}, f32[1024]{0:T(1024)}, u32[]{:S(2)}) copy-start(f32[1024]{0:T(1024)} %param.33) | copy-start | bytes 12292
  133.4 2.0 collective-permute-start
  135.5 14.0 %collective-permute-start.1 = (f32[128,1024]{1,0:T(8,128)S(1)}, f32[128,1024]{1,0:T(8,128)S(1)}, u32[]{:S(2)}, u32[]{:S(2)}) collective-permute-start(f32[128,1024]{1,0:T(8,128)S(1)} %add.91), channel_id=1, source_target_pairs={{0,2},{1,3},{2,0},{3,1},{4,6},{5,7},{6,4},{7,5},{8,10},{9,11},{10,... | collective-permute-start | bytes 1572872 | tf_op jit(solution)/shard_map/ppermute | solution.py:91
  149.7 6.1 %copy-start.9 = (u32[32]{0:T(128)S(1)}, u32[32]{0:T(128)}, u32[]{:S(2)}) copy-start(u32[32]{0:T(128)} %constant.44) | copy-start | bytes 388
  155.7 71.2 %all-gather.2.cloned.1.call-start = ((), (), s32[]{:S(2)}) async-start(), calls=%async_computation.12 | async-start | bytes 1310720 | tf_op jit(solution)/shard_map/all_gather | solution.py:106
  199.6 67.9 %copy-start.1 = (bf16[1024,1024]{1,0:T(8,128)(2,1)S(1)}, bf16[1024,1024]{1,0:T(8,128)(2,1)}, u32[]{:S(2)}) copy-start(bf16[1024,1024]{1,0:T(8,128)(2,1)} %param.27) | copy-start | bytes 6291460
  199.6 66.1 %all-reduce.3.cloned.1.call-start = ((), (), s32[]{:S(2)}) async-start(), calls=%async_computation.13 | async-start | bytes 1048576 | tf_op jit(solution)/shard_map/psum | solution.py:110
Sparse Core Ops, SparseCore 0:
  9.6 22.7 reduce-scatter.6
  34.6 18.2 reduce-scatter.10
  55.2 18.2 reduce-scatter.8
  75.6 20.1 reduce-scatter.12
  97.8 20.0 reduce-scatter.14
  155.8 41.8 reduce-scatter.16
  199.7 27.1 all-gather.1
  232.9 32.7 all-reduce.2
